TPU v7x, 32 devices: a whole 2x2x4 slice. The times are simulated.
32 devices in a mesh: fs: 8 (over z, x), tp: 4 (over y, core).
Axes of the slice: x: 2, y: 2, z: 4, core: 2. Of those that a mesh axis runs over, the one named last changes fastest.
Arguments:
- tokens: bfloat16 [8192, 2048], P('fs', 'tp'), may hold values from -17 to 17
- first_gain: float32 [2048], replicated, may hold values from 0.1 to 1.9
- first_gate: bfloat16 [2048, 5120], P('fs', 'tp'), may hold values from -0.125 to 0.125
- first_up: bfloat16 [2048, 5120], P('fs', 'tp'), may hold values from -0.125 to 0.125
- first_down: bfloat16 [2048, 5120], P('fs', 'tp'), may hold values from -0.078125 to 0.078125
- mix_gain: float32 [2048], replicated, may hold values from 0.1 to 1.9
- mix_input: bfloat16 [2048, 1024], P('fs', 'tp'), may hold values from -0.125 to 0.125
- mix_branch: bfloat16 [2048, 1024], P('fs', 'tp'), may hold values from -0.125 to 0.125
- conv_weight: bfloat16 [4, 1024], P(None, 'tp'), may hold values from -3 to 3
- rate_weight: bfloat16 [16, 64, 64], P('tp'), may hold values from -0.75 to 0.75
- input_weight: bfloat16 [16, 64, 64], P('tp'), may hold values from -0.75 to 0.75
- decay_param: float32 [1024], P('tp'), may hold values from 3 to 11
- decay_shift: float32 [8192, 16], P('fs', 'tp'), may hold values from -1.5 to 0
- mix_output: bfloat16 [2048, 1024], P('fs', 'tp'), may hold values from -0.1875 to 0.1875
- second_gain: float32 [2048], replicated, may hold values from 0.1 to 1.9
- second_gate: bfloat16 [2048, 5120], P('fs', 'tp'), may hold values from -0.125 to 0.125
- second_up: bfloat16 [2048, 5120], P('fs', 'tp'), may hold values from -0.125 to 0.125
- second_down: bfloat16 [2048, 5120], P('fs', 'tp'), may hold values from -0.078125 to 0.078125
- final_gain: float32 [2048], P('tp'), may hold values from 0.1 to 1.9
Outputs:
- output: bfloat16 [8192, 2048], P('fs', 'tp')
All inputs are finite; a program needn't handle non-finite values.
Results may differ from a plain program's by a relative error of at most 0.019.
Values may be sent and summed in bfloat16 or wider, within the bound.
A program may use at most 128 MiB of HBM per device.

v0:
```python
import jax
import jax.numpy as jnp
from jax import lax
from jax.sharding import PartitionSpec as P

D = 2048
HEAD_DIM = 64
CONV = 4
SEQ = 1024
norm_eps = 1e-06
rate_scale = 8.0


def rms_rows(rows, gain):
    values = rows.astype(jnp.float32)
    scale = lax.rsqrt(jnp.mean(values * values, axis=-1, keepdims=True) + norm_eps)
    return (values * scale * gain).astype(jnp.bfloat16)


def full_rows(stream, gain):
    whole = lax.all_gather(stream, "tp", axis=1, tiled=True)
    return rms_rows(whole, gain)


def reduce_back(partial_value):
    return lax.psum_scatter(
        partial_value.astype(jnp.bfloat16), "tp", scatter_dimension=1, tiled=True
    ).astype(jnp.float32)


def contract_last(left, right):
    return lax.dot_general(
        left, right, (((1,), (1,)), ((), ())), preferred_element_type=jnp.float32
    )


def half_step(stream, gain, weight_gate, weight_up, weight_down):
    normed = full_rows(stream, gain)
    whole_gate, whole_up, whole_down = (
        lax.all_gather(weight_gate, "fs", axis=0, tiled=True),
        lax.all_gather(weight_up, "fs", axis=0, tiled=True),
        lax.all_gather(weight_down, "fs", axis=0, tiled=True),
    )
    gate_value = jnp.dot(normed, whole_gate, preferred_element_type=jnp.float32)
    up_value = jnp.dot(normed, whole_up, preferred_element_type=jnp.float32)
    hidden = (jax.nn.silu(gate_value) * up_value).astype(jnp.bfloat16)
    partial_value = contract_last(hidden, whole_down)
    total = reduce_back(partial_value)
    return (stream.astype(jnp.float32) + 0.5 * total).astype(jnp.bfloat16)


def combine_steps(earlier, later):
    return (earlier[0] * later[0], later[0] * earlier[1] + later[1])


def lane_mixer(
    stream,
    gain,
    mix_input,
    mix_branch,
    conv_weight,
    rate_weight,
    input_weight,
    decay_param,
    decay_shift,
    mix_output,
):
    normed = full_rows(stream, gain)
    whole_input, whole_branch, whole_output = (
        lax.all_gather(mix_input, "fs", axis=0, tiled=True),
        lax.all_gather(mix_branch, "fs", axis=0, tiled=True),
        lax.all_gather(mix_output, "fs", axis=0, tiled=True),
    )
    lane_input = jnp.dot(normed, whole_input, preferred_element_type=jnp.float32).astype(
        jnp.bfloat16
    )
    branch_value = jnp.dot(normed, whole_branch, preferred_element_type=jnp.float32)
    width = lane_input.shape[1]
    lanes = lane_input.reshape(-1, SEQ, width).astype(jnp.float32)
    count = lanes.shape[0]
    padded = jnp.pad(lanes, ((0, 0), (CONV - 1, 0), (0, 0)))
    conv_sum = jnp.zeros_like(lanes)
    for offset in range(CONV):
        conv_sum = conv_sum + padded[:, offset : offset + SEQ] * conv_weight[offset].astype(
            jnp.float32
        )
    conv_out = conv_sum.astype(jnp.bfloat16)
    blocks = conv_out.reshape(count, SEQ, -1, HEAD_DIM)
    rate = jax.nn.sigmoid(
        jnp.einsum("nshd,hde->nshe", blocks, rate_weight, preferred_element_type=jnp.float32)
    ).reshape(lanes.shape)
    admit = jax.nn.sigmoid(
        jnp.einsum("nshd,hde->nshe", blocks, input_weight, preferred_element_type=jnp.float32)
    ).reshape(lanes.shape)
    shift = jnp.repeat(decay_shift.reshape(count, SEQ, -1), HEAD_DIM, axis=-1)
    log_decay = rate_scale * rate * jax.nn.log_sigmoid(decay_param) + shift
    drive = jnp.sqrt(-jnp.expm1(2.0 * log_decay)) * admit * conv_out.astype(jnp.float32)
    _, state = lax.associative_scan(combine_steps, (jnp.exp(log_decay), drive), axis=1)
    mixed_lane = (state.reshape(-1, width) * jax.nn.gelu(branch_value)).astype(jnp.bfloat16)
    total = reduce_back(contract_last(mixed_lane, whole_output))
    return (stream.astype(jnp.float32) + total).astype(jnp.bfloat16)


def shards(
    tokens,
    first_gain,
    first_gate,
    first_up,
    first_down,
    mix_gain,
    mix_input,
    mix_branch,
    conv_weight,
    rate_weight,
    input_weight,
    decay_param,
    decay_shift,
    mix_output,
    second_gain,
    second_gate,
    second_up,
    second_down,
    final_gain,
):
    stream = half_step(tokens, first_gain, first_gate, first_up, first_down)
    stream = lane_mixer(
        stream,
        mix_gain,
        mix_input,
        mix_branch,
        conv_weight,
        rate_weight,
        input_weight,
        decay_param,
        decay_shift,
        mix_output,
    )
    stream = half_step(stream, second_gain, second_gate, second_up, second_down)
    values = stream.astype(jnp.float32)
    squares = lax.psum(jnp.sum(values * values, axis=1), "tp")
    scale = lax.rsqrt(squares / D + norm_eps)
    return (values * scale[:, None] * final_gain).astype(jnp.bfloat16)


def solution(mesh):
    return jax.shard_map(
        shards,
        mesh=mesh,
        in_specs=(
            P("fs", "tp"),
            P(),
            P("fs", "tp"),
            P("fs", "tp"),
            P("fs", "tp"),
            P(),
            P("fs", "tp"),
            P("fs", "tp"),
            P(None, "tp"),
            P("tp", None, None),
            P("tp", None, None),
            P("tp"),
            P("fs", "tp"),
            P("fs", "tp"),
            P(),
            P("fs", "tp"),
            P("fs", "tp"),
            P("fs", "tp"),
            P("tp"),
        ),
        out_specs=P("fs", "tp"),
        check_vma=False,
    )
```

profile of v0, /device:TPU:0, one launch (start us, length us, event | category | flops | bytes accessed | tf_op | source)
XLA Modules:
  0.0 989.3 jit_solution(604671720317064304)
XLA Ops:
  9.4 36.7 %all-gather.13.cloned.1.call-done = bf16[1024,2048]{1,0:T(8,128)(2,1)} async-done(((bf16[1024,512]{1,0:T(8,128)(2,1)}), bf16[1024,2048]{1,0:T(8,128)(2,1)}) %all-gather.13.cloned.1.call-update) | async-done | bytes 4194320 | tf_op jit(solution)/shard_map/all_gather | solution.py:21
  46.1 3.1 fusion
  49.2 85.0 %all-gather.15.cloned.1.call-done = bf16[2048,1280]{1,0:T(8,128)(2,1)} async-done(((bf16[256,1280]{1,0:T(8,128)(2,1)}), bf16[2048,1280]{1,0:T(8,128)(2,1)}) %all-gather.15.cloned.1.call-update) | async-done | bytes 5242896 | tf_op jit(solution)/shard_map/all_gather | solution.py:40
  134.2 10.7 %fusion.24 = f32[1024,1280]{1,0:T(8,128)} fusion(bf16[2048,1280]{1,0:T(8,128)(2,1)} %all-gather.15.cloned.1.call-done, bf16[1024,2048]{1,0:T(8,128)(2,1)} %all-gather.13.cloned.1.call-done, f32[2048]{0:T(1024)S(1)} %copy-done.15, f32[1024]{0:T(1024)S(1)} %add_rsqrt_fusion.3), kind=kOutput, calls=%fused_computation.41 | convolution fusion | flops 5377097728 | bytes 14692352 | tf_op jit(solution)/shard_map/dot_general | solution.py:44
  144.9 75.6 %all-gather.17.cloned.1.call-done = bf16[2048,1280]{1,0:T(8,128)(2,1)} async-done(((bf16[256,1280]{1,0:T(8,128)(2,1)}), bf16[2048,1280]{1,0:T(8,128)(2,1)}) %all-gather.17.cloned.1.call-update) | async-done | bytes 5242896 | tf_op jit(solution)/shard_map/all_gather | solution.py:41
  220.5 86.1 %all-gather.19.cloned.1.call-done = bf16[2048,1280]{1,0:T(8,128)(2,1)} async-done(((bf16[256,1280]{1,0:T(8,128)(2,1)}), bf16[2048,1280]{1,0:T(8,128)(2,1)}) %all-gather.19.cloned.1.call-update) | async-done | bytes 5242896 | tf_op jit(solution)/shard_map/all_gather | solution.py:42
  306.6 19.8 %convolution_convert_fusion.2 = bf16[1024,2048]{1,0:T(8,128)(2,1)} fusion(bf16[2048,1280]{1,0:T(8,128)(2,1)} %all-gather.19.cloned.1.call-done, f32[1024,1280]{1,0:T(8,128)} %fusion.24, bf16[2048,1280]{1,0:T(8,128)(2,1)} %all-gather.17.cloned.1.call-done, bf16[1024,2048]{1,0:T(8,128)(2,1)} %all-gather.13.cloned.1.call-done, f32[2048]{0:T(1024)S(1)} %copy-done.15, ...), kind=kOutput, calls=%fused_computation.19 | convolution fusion | flops 10755768320 | bytes 24129536 | tf_op jit(solution)/shard_map/dot_general | solution.py:32
  326.5 42.7 %reduce-scatter.4.cloned.1.call-done = bf16[1024,512]{1,0:T(8,128)(2,1)} async-done(((bf16[1024,2048]{1,0:T(8,128)(2,1)}), bf16[1024,512]{1,0:T(8,128)(2,1)}) %reduce-scatter.4.cloned.1.call-update) | async-done | bytes 1048592 | tf_op jit(solution)/shard_map/reduce_scatter | solution.py:26
  369.2 2.5 add_convert_fusion.2
  375.7 30.7 %all-gather.21.cloned.1.call-done = bf16[1024,2048]{1,0:T(8,128)(2,1)} async-done(((bf16[1024,512]{1,0:T(8,128)(2,1)}), bf16[1024,2048]{1,0:T(8,128)(2,1)}) %all-gather.21.cloned.1.call-update) | async-done | bytes 4194320 | tf_op jit(solution)/shard_map/all_gather | solution.py:21
  406.4 3.1 fusion.3
  409.5 39.3 %all-gather.23.cloned.1.call-done = bf16[2048,256]{1,0:T(8,128)(2,1)} async-done(((bf16[256,256]{1,0:T(8,128)(2,1)}), bf16[2048,256]{1,0:T(8,128)(2,1)}) %all-gather.23.cloned.1.call-update) | async-done | bytes 1048592 | tf_op jit(solution)/shard_map/all_gather | solution.py:70
  448.8 3.8 convolution_convert_fusion.3
  457.1 2.7 fusion.58
  459.8 2.3 slice.263
  462.1 2.1 slice.264
  464.2 2.1 slice.262
  466.3 2.1 slice.266
  555.9 2.8 pad.85
  559.8 9.3 convolution_convert_fusion.1
  569.3 43.3 %reduce-scatter.6.cloned.1.call-done = bf16[1024,512]{1,0:T(8,128)(2,1)} async-done(((bf16[1024,2048]{1,0:T(8,128)(2,1)}), bf16[1024,512]{1,0:T(8,128)(2,1)}) %reduce-scatter.6.cloned.1.call-update) | async-done | bytes 1048592 | tf_op jit(solution)/shard_map/reduce_scatter | solution.py:26
  612.5 2.5 add_convert_fusion.1
  617.0 32.7 %all-gather.29.cloned.1.call-done = bf16[1024,2048]{1,0:T(8,128)(2,1)} async-done(((bf16[1024,512]{1,0:T(8,128)(2,1)}), bf16[1024,2048]{1,0:T(8,128)(2,1)}) %all-gather.29.cloned.1.call-update) | async-done | bytes 4194320 | tf_op jit(solution)/shard_map/all_gather | solution.py:21
  649.7 3.1 fusion.6
  652.7 84.9 %all-gather.31.cloned.1.call-done = bf16[2048,1280]{1,0:T(8,128)(2,1)} async-done(((bf16[256,1280]{1,0:T(8,128)(2,1)}), bf16[2048,1280]{1,0:T(8,128)(2,1)}) %all-gather.31.cloned.1.call-update) | async-done | bytes 5242896 | tf_op jit(solution)/shard_map/all_gather | solution.py:40
  737.6 10.7 %fusion.19 = f32[1024,1280]{1,0:T(8,128)} fusion(bf16[2048,1280]{1,0:T(8,128)(2,1)} %all-gather.31.cloned.1.call-done, bf16[1024,2048]{1,0:T(8,128)(2,1)} %all-gather.29.cloned.1.call-done, f32[2048]{0:T(1024)S(1)} %copy-done.18, f32[1024]{0:T(1024)S(1)} %add_rsqrt_fusion.1), kind=kOutput, calls=%fused_computation.40 | convolution fusion | flops 5377097728 | bytes 14692352 | tf_op jit(solution)/shard_map/dot_general | solution.py:44
  748.3 75.6 %all-gather.33.cloned.1.call-done = bf16[2048,1280]{1,0:T(8,128)(2,1)} async-done(((bf16[256,1280]{1,0:T(8,128)(2,1)}), bf16[2048,1280]{1,0:T(8,128)(2,1)}) %all-gather.33.cloned.1.call-update) | async-done | bytes 5242896 | tf_op jit(solution)/shard_map/all_gather | solution.py:41
  823.9 86.1 %all-gather.35.cloned.1.call-done = bf16[2048,1280]{1,0:T(8,128)(2,1)} async-done(((bf16[256,1280]{1,0:T(8,128)(2,1)}), bf16[2048,1280]{1,0:T(8,128)(2,1)}) %all-gather.35.cloned.1.call-update) | async-done | bytes 5242896 | tf_op jit(solution)/shard_map/all_gather | solution.py:42
  910.0 19.8 %convolution_convert_fusion = bf16[1024,2048]{1,0:T(8,128)(2,1)} fusion(bf16[2048,1280]{1,0:T(8,128)(2,1)} %all-gather.35.cloned.1.call-done, f32[1024,1280]{1,0:T(8,128)} %fusion.19, bf16[2048,1280]{1,0:T(8,128)(2,1)} %all-gather.33.cloned.1.call-done, bf16[1024,2048]{1,0:T(8,128)(2,1)} %all-gather.29.cloned.1.call-done, f32[2048]{0:T(1024)S(1)} %copy-done.18, ...), kind=kOutput, calls=%fused_computation.17 | convolution fusion | flops 10755768320 | bytes 24129536 | tf_op jit(solution)/shard_map/dot_general | solution.py:32
  929.9 42.8 %reduce-scatter.8.cloned.1.call-done = bf16[1024,512]{1,0:T(8,128)(2,1)} async-done(((bf16[1024,2048]{1,0:T(8,128)(2,1)}), bf16[1024,512]{1,0:T(8,128)(2,1)}) %reduce-scatter.8.cloned.1.call-update) | async-done | bytes 1048592 | tf_op jit(solution)/shard_map/reduce_scatter | solution.py:26
  974.3 5.8 psum.7
  980.1 2.7 fusion.11
  (196 shorter events, 103.3 us)
Async XLA Ops:
  6.5 446.9 %copy-start = (bf16[4,64,64]{2,1,0:T(8,128)(2,1)S(1)}, bf16[4,64,64]{2,1,0:T(8,128)(2,1)}, u32[]{:S(2)}) copy-start(bf16[4,64,64]{2,1,0:T(8,128)(2,1)} %param.28) | copy-start | bytes 98308
  6.5 127.7 %copy-start.15 = (f32[2048]{0:T(1024)S(1)}, f32[2048]{0:T(1024)}, u32[]{:S(2)}) copy-start(f32[2048]{0:T(1024)} %param.20) | copy-start | bytes 24580
  6.5 39.6 %all-gather.13.cloned.1.call-start = ((), (), s32[]{:S(2)}) async-start(), calls=%async_computation.3 | async-start | bytes 5242880 | tf_op jit(solution)/shard_map/all_gather | solution.py:21
  7.3 126.9 %all-gather.15.cloned.1.call-start = ((), (), s32[]{:S(2)}) async-start(), calls=%async_computation.4 | async-start | bytes 5898240 | tf_op jit(solution)/shard_map/all_gather | solution.py:40
  8.0 212.5 %all-gather.17.cloned.1.call-start = ((), (), s32[]{:S(2)}) async-start(), calls=%async_computation.5 | async-start | bytes 5898240 | tf_op jit(solution)/shard_map/all_gather | solution.py:41
  8.7 297.9 %all-gather.19.cloned.1.call-start = ((), (), s32[]{:S(2)}) async-start(), calls=%async_computation.6 | async-start | bytes 5898240 | tf_op jit(solution)/shard_map/all_gather | solution.py:42
  9.3 359.9 %reduce-scatter.4.cloned.1.call-start = ((), (), s32[]{:S(2)}) async-start(), calls=%async_computation.7 | async-start | bytes 5242880 | tf_op jit(solution)/shard_map/reduce_scatter | solution.py:26
  144.9 224.3 %copy-start.4 = (bf16[1024,512]{1,0:T(8,128)(2,1)S(1)}, bf16[1024,512]{1,0:T(8,128)(2,1)}, u32[]{:S(2)}) copy-start(bf16[1024,512]{1,0:T(8,128)(2,1)} %param.19) | copy-start | bytes 3145732
  326.4 47.8 %copy-start.7 = (bf16[4,256]{1,0:T(4,128)(2,1)S(1)}, bf16[4,256]{1,0:T(4,128)(2,1)}, u32[]{:S(2)}) copy-start(bf16[4,256]{1,0:T(4,128)(2,1)} %param.27) | copy-start | bytes 6148
  326.4 47.8 %copy-start.6 = (f32[1024,4]{0,1:T(4,128)S(1)}, f32[1024,4]{0,1:T(4,128)}, u32[]{:S(2)}) copy-start(f32[1024,4]{0,1:T(4,128)} %param.31) | copy-start | bytes 49156
  326.4 49.3 %copy-start.13 = (f32[256]{0:T(256)S(1)}, f32[256]{0:T(256)}, u32[]{:S(2)}) copy-start(f32[256]{0:T(256)} %param.30) | copy-start | bytes 3076
  326.4 122.4 %copy-start.16 = (f32[2048]{0:T(1024)S(1)}, f32[2048]{0:T(1024)}, u32[]{:S(2)}) copy-start(f32[2048]{0:T(1024)} %param.24) | copy-start | bytes 24580
  326.5 79.9 %all-gather.21.cloned.1.call-start = ((), (), s32[]{:S(2)}) async-start(), calls=%async_computation.8 | async-start | bytes 5242880 | tf_op jit(solution)/shard_map/all_gather | solution.py:21
  371.8 77.0 %all-gather.23.cloned.1.call-start = ((), (), s32[]{:S(2)}) async-start(), calls=%async_computation.9 | async-start | bytes 1179648 | tf_op jit(solution)/shard_map/all_gather | solution.py:70
  372.5 186.5 %all-gather.25.cloned.1.call-start = ((), (), s32[]{:S(2)}) async-start(), calls=%async_computation.10 | async-start | bytes 1179648 | tf_op jit(solution)/shard_map/all_gather | solution.py:71
  373.3 185.8 %all-gather.27.cloned.1.call-start = ((), (), s32[]{:S(2)}) async-start(), calls=%async_computation.11 | async-start | bytes 1179648 | tf_op jit(solution)/shard_map/all_gather | solution.py:72
  374.0 238.5 %reduce-scatter.6.cloned.1.call-start = ((), (), s32[]{:S(2)}) async-start(), calls=%async_computation.12 | async-start | bytes 5242880 | tf_op jit(solution)/shard_map/reduce_scatter | solution.py:26
  409.5 43.1 %copy-start.10 = (f32[1024]{0:T(1024)}, f32[1024]{0:T(1024)S(1)}, u32[]{:S(2)}) copy-start(f32[1024]{0:T(1024)S(1)} %add_rsqrt_fusion.2) | copy-start | bytes 12292
  543.6 12.0 %copy-start.9 = (f32[1,1,256]{2,1,0:T(1,128)S(1)}, f32[1,1,256]{2,1,0:T(1,128)}, u32[]{:S(2)}) copy-start(f32[1,1,256]{2,1,0:T(1,128)} %slice.336) | copy-start | bytes 3076
  554.4 4.3 copy-start.8
  555.6 3.5 copy-start.11
  555.6 3.5 copy-start.17
  559.0 53.6 %copy-start.3 = (bf16[1024,512]{1,0:T(8,128)(2,1)S(1)}, bf16[1024,512]{1,0:T(8,128)(2,1)}, u32[]{:S(2)}) copy-start(bf16[1024,512]{1,0:T(8,128)(2,1)} %add_convert_fusion.2) | copy-start | bytes 3145732
  569.2 168.4 %copy-start.18 = (f32[2048]{0:T(1024)S(1)}, f32[2048]{0:T(1024)}, u32[]{:S(2)}) copy-start(f32[2048]{0:T(1024)} %param.33) | copy-start | bytes 24580
  569.2 80.4 %all-gather.29.cloned.1.call-start = ((), (), s32[]{:S(2)}) async-start(), calls=%async_computation.13 | async-start | bytes 5242880 | tf_op jit(solution)/shard_map/all_gather | solution.py:21
  615.0 122.6 %all-gather.31.cloned.1.call-start = ((), (), s32[]{:S(2)}) async-start(), calls=%async_computation.14 | async-start | bytes 5898240 | tf_op jit(solution)/shard_map/all_gather | solution.py:40
  615.6 208.3 %all-gather.33.cloned.1.call-start = ((), (), s32[]{:S(2)}) async-start(), calls=%async_computation.15 | async-start | bytes 5898240 | tf_op jit(solution)/shard_map/all_gather | solution.py:41
  616.4 293.7 %all-gather.35.cloned.1.call-start = ((), (), s32[]{:S(2)}) async-start(), calls=%async_computation.16 | async-start | bytes 5898240 | tf_op jit(solution)/shard_map/all_gather | solution.py:42
  616.9 355.7 %reduce-scatter.8.cloned.1.call-start = ((), (), s32[]{:S(2)}) async-start(), calls=%async_computation.17 | async-start | bytes 5242880 | tf_op jit(solution)/shard_map/reduce_scatter | solution.py:26
  748.3 224.3 %copy-start.2 = (bf16[1024,512]{1,0:T(8,128)(2,1)S(1)}, bf16[1024,512]{1,0:T(8,128)(2,1)}, u32[]{:S(2)}) copy-start(bf16[1024,512]{1,0:T(8,128)(2,1)} %add_convert_fusion.1) | copy-start | bytes 3145732
  910.0 72.8 %copy-start.1 = (bf16[4,64,64]{2,1,0:T(8,128)(2,1)S(1)}, bf16[4,64,64]{2,1,0:T(8,128)(2,1)}, u32[]{:S(2)}) copy-start(bf16[4,64,64]{2,1,0:T(8,128)(2,1)} %param.28) | copy-start | bytes 98308
  929.9 50.3 %copy-start.12 = (f32[512]{0:T(512)S(1)}, f32[512]{0:T(512)}, u32[]{:S(2)}) copy-start(f32[512]{0:T(512)} %param.37) | copy-start | bytes 6148
  (2 other events, 3.8 us)
Sparse Core Ops, SparseCore 0:
  8.9 37.1 all-gather.12
  48.3 85.8 all-gather.14
  136.4 84.0 all-gather.16
  222.5 84.0 all-gather.18
  326.6 42.6 reduce-scatter.3
  371.9 34.4 all-gather.20
  408.5 40.2 all-gather.22
  450.9 38.9 all-gather.24
  492.1 38.9 all-gather.26
  569.3 43.1 reduce-scatter.5
  615.2 34.4 all-gather.28
  651.7 85.8 all-gather.30
  739.8 84.0 all-gather.32
  825.9 84.0 all-gather.34
  930.0 42.5 reduce-scatter.7
where the time goes:
time: 992 us; the launch traced here: 989 us
  waiting for transfers between devices  768 us (77%)
  local copies, waits for them, and re-layouts  78.1 us (8%)
  matrix products  75.1 us (8%)
  other arithmetic  47.8 us (5%)
  between operations  13.8 us (1%)
    all_gather x2, waiting for transfers between devices, half_step(): lax.all_gather(weight_down, 'fs', axis=0, tiled=True)  172 us
    all_gather x2, waiting for transfers between devices, half_step(): lax.all_gather(weight_gate, 'fs', axis=0, tiled=True)  170 us
    all_gather x2, waiting for transfers between devices, half_step(): lax.all_gather(weight_up, 'fs', axis=0, tiled=True)  151 us
    reduce_scatter x3, waiting for transfers between devices, reduce_back(): lax.psum_scatter(partial_value.astype(jnp.bfloat16), 'tp', scatter_dimens...  129 us
    all_gather x3, waiting for transfers between devices, full_rows(): whole = lax.all_gather(stream, 'tp', axis=1, tiled=True)  100 us
    slice x60, local copies, waits for them, and re-layouts, lane_mixer(): lax.associative_scan(combine_steps, (jnp.exp(log_decay), drive), axis=1)  69.1 us
    dot_general x3, matrix products, contract_last(): lax.dot_general(left, right, (((1,), (1,)), ((), ())), preferred_element_...  48.9 us
    all_gather x1, waiting for transfers between devices, lane_mixer(): lax.all_gather(mix_input, 'fs', axis=0, tiled=True)  39.3 us
  transfers between devices with their start and end apart: 15, of which 13 were waited for; matrix products, arithmetic and copies ran while one was open for 14% of the time, Pallas kernels for 0%

commit v1 on v0

--- a/solution.py
+++ b/solution.py
@@ -18,7 +18,12 @@
 
 
 def full_rows(stream, gain):
-    whole = lax.all_gather(stream, "tp", axis=1, tiled=True)
+    ring = [stream]
+    for hop in range(3):
+        ring.append(lax.ppermute(ring[-1], "tp", [(dev, (dev + 1) % 4) for dev in range(4)]))
+    whole = jnp.roll(
+        jnp.concatenate(ring[::-1], axis=1), (lax.axis_index("tp") + 1) * ring[0].shape[1], axis=1
+    )
     return rms_rows(whole, gain)
 
 

time: 992 us -> 920 us (0.927)
  waiting for transfers between devices: 768 us -> 637 us
  other arithmetic: 47.8 us -> 75.3 us
  starting transfers between devices: 0.73 us -> 12.3 us
  local copies, waits for them, and re-layouts: 78.1 us -> 89.2 us
    ppermute x0 -> x9, waiting for transfers between devices: none -> 116 us  [full_rows(): lax.ppermute(ring[-1], 'tp', [(dev, (dev + 1) % 4) for dev in range(4)])]
    all_gather x2, waiting for transfers between devices: 170 us -> 65.1 us  [half_step(): lax.all_gather(weight_gate, 'fs', axis=0, tiled=True)]
    all_gather x3 -> x0, waiting for transfers between devices: 100 us -> none  [full_rows(): whole = lax.all_gather(stream, 'tp', axis=1, tiled=True)]
    all_gather x1, waiting for transfers between devices: 39.3 us -> 0.02 us  [lane_mixer(): lax.all_gather(mix_input, 'fs', axis=0, tiled=True)]
    reduce_sum x3, other arithmetic: 9.21 us -> 36.1 us  [rms_rows(): jnp.mean(values * values, axis=-1, keepdims=True) + norm_eps]
    reduce_scatter x3, starting transfers between devices: 0.3 us -> 11.3 us  [reduce_back(): lax.psum_scatter(partial_value.astype(jnp.bfloat16), 'tp', scatter_dimens...]
  transfers between devices with their start and end apart: 15 -> 21, of which waited for: 13 -> 18; matrix products, arithmetic and copies ran while one was open for 14% -> 20% of each run, Pallas kernels for 0% -> 0%
where the time goes in v1:
time: 920 us; the launch traced here: 909 us
  waiting for transfers between devices  637 us (69%)
  local copies, waits for them, and re-layouts  89.2 us (10%)
  matrix products  75.4 us (8%)
  other arithmetic  75.3 us (8%)
  between operations  14.4 us (2%)
  starting transfers between devices  12.3 us (1%)
    all_gather x2, waiting for transfers between devices, half_step(): lax.all_gather(weight_down, 'fs', axis=0, tiled=True)  173 us
    all_gather x2, waiting for transfers between devices, half_step(): lax.all_gather(weight_up, 'fs', axis=0, tiled=True)  151 us
    reduce_scatter x3, waiting for transfers between devices, reduce_back(): lax.psum_scatter(partial_value.astype(jnp.bfloat16), 'tp', scatter_dimens...  127 us
    ppermute x9, waiting for transfers between devices, full_rows(): lax.ppermute(ring[-1], 'tp', [(dev, (dev + 1) % 4) for dev in range(4)])  116 us
    slice x60, local copies, waits for them, and re-layouts, lane_mixer(): lax.associative_scan(combine_steps, (jnp.exp(log_decay), drive), axis=1)  78.1 us
    all_gather x2, waiting for transfers between devices, half_step(): lax.all_gather(weight_gate, 'fs', axis=0, tiled=True)  65.1 us
    dot_general x3, matrix products, contract_last(): lax.dot_general(left, right, (((1,), (1,)), ((), ())), preferred_element_...  49.2 us
    reduce_sum x3, other arithmetic, rms_rows(): jnp.mean(values * values, axis=-1, keepdims=True) + norm_eps  36.1 us
  transfers between devices with their start and end apart: 21, of which 18 were waited for; matrix products, arithmetic and copies ran while one was open for 20% of the time, Pallas kernels for 0%

profile of v1, /device:TPU:0, one launch (start us, length us, event | category | flops | bytes accessed | tf_op | source)
XLA Modules:
  0.0 909.1 jit_solution(5547294855482920669)
XLA Ops:
  9.3 14.6 %collective-permute-done = bf16[1024,512]{1,0:T(8,128)(2,1)S(1)} collective-permute-done((bf16[1024,512]{1,0:T(8,128)(2,1)}, bf16[1024,512]{1,0:T(8,128)(2,1)S(1)}, u32[]{:S(2)}, u32[]{:S(2)}) %collective-permute-start) | collective-permute-done | bytes 1048608 | tf_op jit(solution)/shard_map/ppermute | solution.py:23
  24.0 14.2 %collective-permute-done.1 = bf16[1024,512]{1,0:T(8,128)(2,1)S(1)} collective-permute-done((bf16[1024,512]{1,0:T(8,128)(2,1)S(1)}, bf16[1024,512]{1,0:T(8,128)(2,1)S(1)}, u32[]{:S(2)}, u32[]{:S(2)}) %collective-permute-start.1) | collective-permute-done | bytes 1048608 | tf_op jit(solution)/shard_map/ppermute | solution.py:23
  38.2 14.2 %collective-permute-done.2 = bf16[1024,512]{1,0:T(8,128)(2,1)S(1)} collective-permute-done((bf16[1024,512]{1,0:T(8,128)(2,1)S(1)}, bf16[1024,512]{1,0:T(8,128)(2,1)S(1)}, u32[]{:S(2)}, u32[]{:S(2)}) %collective-permute-start.2) | collective-permute-done | bytes 1048608 | tf_op jit(solution)/shard_map/ppermute | solution.py:23
  52.4 12.0 %fusion = (f32[1024]{0:T(1024)S(1)}, bf16[1024,2048]{1,0:T(8,128)(2,1)}) fusion(s32[]{:T(128)S(6)} %select_n.21, bf16[1024,512]{1,0:T(8,128)(2,1)} %param.21, bf16[1024,512]{1,0:T(8,128)(2,1)S(1)} %collective-permute-done, bf16[1024,512]{1,0:T(8,128)(2,1)S(1)} %collective-permute-done.1, bf16[1024,512]{1,0:T(8,128)(2,1)S(1)} %collective-permute-done.2), kind=kLoop, calls=%fused_computation.6 | loop fusion | flops 39844864 | bytes 8392708 | tf_op jit(solution)/shard_map/reduce_sum | solution.py:16
  64.4 33.7 %all-gather.10.cloned.1.call-done = bf16[2048,1280]{1,0:T(8,128)(2,1)} async-done(((bf16[256,1280]{1,0:T(8,128)(2,1)}), bf16[2048,1280]{1,0:T(8,128)(2,1)}) %all-gather.10.cloned.1.call-update) | async-done | bytes 5242896 | tf_op jit(solution)/shard_map/all_gather | solution.py:45
  98.2 10.7 %fusion.45 = f32[1024,1280]{1,0:T(8,128)} fusion(bf16[2048,1280]{1,0:T(8,128)(2,1)} %all-gather.10.cloned.1.call-done, bf16[1024,2048]{1,0:T(8,128)(2,1)} %get-tuple-element.11, f32[2048]{0:T(1024)S(1)} %copy-done.14, f32[1024]{0:T(1024)S(1)} %add_rsqrt_fusion.3), kind=kOutput, calls=%fused_computation.86 | convolution fusion | flops 5377097728 | bytes 14692352 | tf_op jit(solution)/shard_map/dot_general | solution.py:49
  108.8 75.6 %all-gather.12.cloned.1.call-done = bf16[2048,1280]{1,0:T(8,128)(2,1)} async-done(((bf16[256,1280]{1,0:T(8,128)(2,1)}), bf16[2048,1280]{1,0:T(8,128)(2,1)}) %all-gather.12.cloned.1.call-update) | async-done | bytes 5242896 | tf_op jit(solution)/shard_map/all_gather | solution.py:46
  184.4 86.3 %all-gather.14.cloned.1.call-done = bf16[2048,1280]{1,0:T(8,128)(2,1)} async-done(((bf16[256,1280]{1,0:T(8,128)(2,1)}), bf16[2048,1280]{1,0:T(8,128)(2,1)}) %all-gather.14.cloned.1.call-update) | async-done | bytes 5242896 | tf_op jit(solution)/shard_map/all_gather | solution.py:47
  270.7 19.8 %convolution_convert_fusion.2 = bf16[1024,2048]{1,0:T(8,128)(2,1)} fusion(bf16[2048,1280]{1,0:T(8,128)(2,1)} %all-gather.14.cloned.1.call-done, f32[1024,1280]{1,0:T(8,128)} %fusion.45, bf16[2048,1280]{1,0:T(8,128)(2,1)} %all-gather.12.cloned.1.call-done, bf16[1024,2048]{1,0:T(8,128)(2,1)} %get-tuple-element.11, f32[2048]{0:T(1024)S(1)} %copy-done.14, ...), kind=kOutput, calls=%fused_computation.64 | convolution fusion | flops 10755768320 | bytes 24129536 | tf_op jit(solution)/shard_map/dot_general | solution.py:37
  291.2 42.1 %reduce-scatter.4.cloned.1.call-done = bf16[1024,512]{1,0:T(8,128)(2,1)} async-done(((bf16[1024,2048]{1,0:T(8,128)(2,1)}), bf16[1024,512]{1,0:T(8,128)(2,1)}) %reduce-scatter.4.cloned.1.call-update) | async-done | bytes 1048592 | tf_op jit(solution)/shard_map/reduce_scatter | solution.py:31
  335.0 14.1 %collective-permute-done.3 = bf16[1024,512]{1,0:T(8,128)(2,1)S(1)} collective-permute-done((bf16[1024,512]{1,0:T(8,128)(2,1)S(1)}, bf16[1024,512]{1,0:T(8,128)(2,1)S(1)}, u32[]{:S(2)}, u32[]{:S(2)}) %collective-permute-start.3) | collective-permute-done | bytes 1048608 | tf_op jit(solution)/shard_map/ppermute | solution.py:23
  349.1 14.3 %collective-permute-done.4 = bf16[1024,512]{1,0:T(8,128)(2,1)} collective-permute-done((bf16[1024,512]{1,0:T(8,128)(2,1)S(1)}, bf16[1024,512]{1,0:T(8,128)(2,1)}, u32[]{:S(2)}, u32[]{:S(2)}) %collective-permute-start.4) | collective-permute-done | bytes 1048608 | tf_op jit(solution)/shard_map/ppermute | solution.py:23
  363.5 11.2 %reduce-scatter.6.cloned.1.call-start = ((), (), s32[]{:S(2)}) async-start(), calls=%async_computation.10 | async-start | bytes 5242880 | tf_op jit(solution)/shard_map/reduce_scatter | solution.py:31
  378.0 11.7 %fusion.3 = (f32[1024]{0:T(1024)S(1)}, bf16[1024,2048]{1,0:T(8,128)(2,1)}) fusion(s32[]{:T(128)S(6)} %select_n.21, bf16[1024,512]{1,0:T(8,128)(2,1)S(1)} %add_convert_fusion.2, bf16[1024,512]{1,0:T(8,128)(2,1)S(1)} %collective-permute-done.3, bf16[1024,512]{1,0:T(8,128)(2,1)} %collective-permute-done.4, bf16[1024,512]{1,0:T(8,128)(2,1)} %collective-permute-done.5), kind=kLoop, calls=%fused_computation.9 | loop fusion | flops 39844864 | bytes 8392708 | tf_op jit(solution)/shard_map/reduce_sum | solution.py:16
  389.7 3.8 convolution_convert_fusion.3
  398.1 2.8 fusion.79
  409.2 2.7 fusion.101
  509.5 4.6 pad.85
  514.5 9.6 %convolution_convert_fusion.1 = bf16[1024,2048]{1,0:T(8,128)(2,1)} fusion(bf16[2048,256]{1,0:T(8,128)(2,1)} %all-gather.20.cloned.1.call-done, bf16[2048,256]{1,0:T(8,128)(2,1)} %all-gather.18.cloned.1.call-done, bf16[1024,2048]{1,0:T(8,128)(2,1)} %get-tuple-element.9, f32[2048]{0:T(1024)S(1)} %copy-done.16, f32[1024]{0:T(1024)S(1)} %copy-done.10, ...), kind=kOutput, calls=%fused_computation.63 | convolution fusion | flops 2160852992 | bytes 12595200 | tf_op jit(solution)/shard_map/dot_general | solution.py:37
  526.2 42.4 %reduce-scatter.6.cloned.1.call-done = bf16[1024,512]{1,0:T(8,128)(2,1)} async-done(((bf16[1024,2048]{1,0:T(8,128)(2,1)}), bf16[1024,512]{1,0:T(8,128)(2,1)}) %reduce-scatter.6.cloned.1.call-update) | async-done | bytes 1048592 | tf_op jit(solution)/shard_map/reduce_scatter | solution.py:31
  570.2 14.2 %collective-permute-done.6 = bf16[1024,512]{1,0:T(8,128)(2,1)S(1)} collective-permute-done((bf16[1024,512]{1,0:T(8,128)(2,1)S(1)}, bf16[1024,512]{1,0:T(8,128)(2,1)S(1)}, u32[]{:S(2)}, u32[]{:S(2)}) %collective-permute-start.6) | collective-permute-done | bytes 1048608 | tf_op jit(solution)/shard_map/ppermute | solution.py:23
  584.4 14.2 %collective-permute-done.7 = bf16[1024,512]{1,0:T(8,128)(2,1)S(1)} collective-permute-done((bf16[1024,512]{1,0:T(8,128)(2,1)S(1)}, bf16[1024,512]{1,0:T(8,128)(2,1)S(1)}, u32[]{:S(2)}, u32[]{:S(2)}) %collective-permute-start.7) | collective-permute-done | bytes 1048608 | tf_op jit(solution)/shard_map/ppermute | solution.py:23
  598.7 14.2 %collective-permute-done.8 = bf16[1024,512]{1,0:T(8,128)(2,1)S(1)} collective-permute-done((bf16[1024,512]{1,0:T(8,128)(2,1)S(1)}, bf16[1024,512]{1,0:T(8,128)(2,1)S(1)}, u32[]{:S(2)}, u32[]{:S(2)}) %collective-permute-start.8) | collective-permute-done | bytes 1048608 | tf_op jit(solution)/shard_map/ppermute | solution.py:23
  612.9 12.5 %fusion.6 = (f32[1024]{0:T(1024)S(1)}, bf16[1024,2048]{1,0:T(8,128)(2,1)}) fusion(s32[]{:T(128)S(6)} %select_n.21, bf16[1024,512]{1,0:T(8,128)(2,1)S(1)} %add_convert_fusion.1, bf16[1024,512]{1,0:T(8,128)(2,1)S(1)} %collective-permute-done.6, bf16[1024,512]{1,0:T(8,128)(2,1)S(1)} %collective-permute-done.7, bf16[1024,512]{1,0:T(8,128)(2,1)S(1)} %collective-permute-done.8), kind=kLoop, calls=%fused_computation.12 | loop fusion | flops 39844864 | bytes 8392708 | tf_op jit(solution)/shard_map/reduce_sum | solution.py:16
  625.3 31.4 %all-gather.22.cloned.1.call-done = bf16[2048,1280]{1,0:T(8,128)(2,1)} async-done(((bf16[256,1280]{1,0:T(8,128)(2,1)}), bf16[2048,1280]{1,0:T(8,128)(2,1)}) %all-gather.22.cloned.1.call-update) | async-done | bytes 5242896 | tf_op jit(solution)/shard_map/all_gather | solution.py:45
  656.7 10.8 %fusion.40 = f32[1024,1280]{1,0:T(8,128)} fusion(bf16[2048,1280]{1,0:T(8,128)(2,1)} %all-gather.22.cloned.1.call-done, bf16[1024,2048]{1,0:T(8,128)(2,1)} %get-tuple-element.7, f32[2048]{0:T(1024)S(1)} %copy-done.17, f32[1024]{0:T(1024)S(1)} %add_rsqrt_fusion.1), kind=kOutput, calls=%fused_computation.85 | convolution fusion | flops 5377097728 | bytes 14692352 | tf_op jit(solution)/shard_map/dot_general | solution.py:49
  667.5 75.4 %all-gather.24.cloned.1.call-done = bf16[2048,1280]{1,0:T(8,128)(2,1)} async-done(((bf16[256,1280]{1,0:T(8,128)(2,1)}), bf16[2048,1280]{1,0:T(8,128)(2,1)}) %all-gather.24.cloned.1.call-update) | async-done | bytes 5242896 | tf_op jit(solution)/shard_map/all_gather | solution.py:46
  742.9 86.3 %all-gather.26.cloned.1.call-done = bf16[2048,1280]{1,0:T(8,128)(2,1)} async-done(((bf16[256,1280]{1,0:T(8,128)(2,1)}), bf16[2048,1280]{1,0:T(8,128)(2,1)}) %all-gather.26.cloned.1.call-update) | async-done | bytes 5242896 | tf_op jit(solution)/shard_map/all_gather | solution.py:47
  829.2 19.8 %convolution_convert_fusion = bf16[1024,2048]{1,0:T(8,128)(2,1)} fusion(bf16[2048,1280]{1,0:T(8,128)(2,1)} %all-gather.26.cloned.1.call-done, f32[1024,1280]{1,0:T(8,128)} %fusion.40, bf16[2048,1280]{1,0:T(8,128)(2,1)} %all-gather.24.cloned.1.call-done, bf16[1024,2048]{1,0:T(8,128)(2,1)} %get-tuple-element.7, f32[2048]{0:T(1024)S(1)} %copy-done.17, ...), kind=kOutput, calls=%fused_computation.62 | convolution fusion | flops 10755768320 | bytes 24129536 | tf_op jit(solution)/shard_map/dot_general | solution.py:37
  849.0 42.8 %reduce-scatter.8.cloned.1.call-done = bf16[1024,512]{1,0:T(8,128)(2,1)} async-done(((bf16[1024,2048]{1,0:T(8,128)(2,1)}), bf16[1024,512]{1,0:T(8,128)(2,1)}) %reduce-scatter.8.cloned.1.call-update) | async-done | bytes 1048592 | tf_op jit(solution)/shard_map/reduce_scatter | solution.py:31
  893.5 5.8 psum.7
  899.2 2.7 fusion.32
  (203 shorter events, 124.3 us)
Async XLA Ops:
  6.5 387.8 %copy-start = (bf16[4,64,64]{2,1,0:T(8,128)(2,1)S(1)}, bf16[4,64,64]{2,1,0:T(8,128)(2,1)}, u32[]{:S(2)}) copy-start(bf16[4,64,64]{2,1,0:T(8,128)(2,1)} %param.30) | copy-start | bytes 98308
  6.5 91.6 %copy-start.14 = (f32[2048]{0:T(1024)S(1)}, f32[2048]{0:T(1024)}, u32[]{:S(2)}) copy-start(f32[2048]{0:T(1024)} %param.22) | copy-start | bytes 24580
  6.5 91.6 %all-gather.10.cloned.1.call-start = ((), (), s32[]{:S(2)}) async-start(), calls=%async_computation.3 | async-start | bytes 5898240 | tf_op jit(solution)/shard_map/all_gather | solution.py:45
  7.3 177.2 %all-gather.12.cloned.1.call-start = ((), (), s32[]{:S(2)}) async-start(), calls=%async_computation.4 | async-start | bytes 5898240 | tf_op jit(solution)/shard_map/all_gather | solution.py:46
  8.0 262.7 %all-gather.14.cloned.1.call-start = ((), (), s32[]{:S(2)}) async-start(), calls=%async_computation.5 | async-start | bytes 5898240 | tf_op jit(solution)/shard_map/all_gather | solution.py:47
  8.7 324.6 %reduce-scatter.4.cloned.1.call-start = ((), (), s32[]{:S(2)}) async-start(), calls=%async_computation.6 | async-start | bytes 5242880 | tf_op jit(solution)/shard_map/reduce_scatter | solution.py:31
  8.8 15.2 %collective-permute-start = (bf16[1024,512]{1,0:T(8,128)(2,1)}, bf16[1024,512]{1,0:T(8,128)(2,1)S(1)}, u32[]{:S(2)}, u32[]{:S(2)}) collective-permute-start(bf16[1024,512]{1,0:T(8,128)(2,1)} %param.21), channel_id=1, source_target_pairs={{0,1},{1,2},{2,3},{3,0},{4,5},{5,6},{6,7},{7,4},{8,9},{9,10},{10,1... | collective-permute-start | bytes 3145736 | tf_op jit(solution)/shard_map/ppermute | solution.py:23
  24.0 14.2 %collective-permute-start.1 = (bf16[1024,512]{1,0:T(8,128)(2,1)S(1)}, bf16[1024,512]{1,0:T(8,128)(2,1)S(1)}, u32[]{:S(2)}, u32[]{:S(2)}) collective-permute-start(bf16[1024,512]{1,0:T(8,128)(2,1)S(1)} %collective-permute-done), channel_id=1, source_target_pairs={{0,1},{1,2},{2,3},{3,0},{4,5},{5,6},{6,7},{7,4},{8,9},{9,10},{10,1... | collective-permute-start | bytes 3145736 | tf_op jit(solution)/shard_map/ppermute | solution.py:23
  38.2 14.2 %collective-permute-start.2 = (bf16[1024,512]{1,0:T(8,128)(2,1)S(1)}, bf16[1024,512]{1,0:T(8,128)(2,1)S(1)}, u32[]{:S(2)}, u32[]{:S(2)}) collective-permute-start(bf16[1024,512]{1,0:T(8,128)(2,1)S(1)} %collective-permute-done.1), channel_id=1, source_target_pairs={{0,1},{1,2},{2,3},{3,0},{4,5},{5,6},{6,7},{7,4},{8,9},{9,10},{10,1... | collective-permute-start | bytes 3145736 | tf_op jit(solution)/shard_map/ppermute | solution.py:23
  108.8 224.5 %copy-start.3 = (bf16[1024,512]{1,0:T(8,128)(2,1)S(1)}, bf16[1024,512]{1,0:T(8,128)(2,1)}, u32[]{:S(2)}) copy-start(bf16[1024,512]{1,0:T(8,128)(2,1)} %param.21) | copy-start | bytes 3145732
  290.5 84.2 %copy-start.5 = (f32[1024,4]{0,1:T(4,128)S(1)}, f32[1024,4]{0,1:T(4,128)}, u32[]{:S(2)}) copy-start(f32[1024,4]{0,1:T(4,128)} %param.33) | copy-start | bytes 49156
  290.5 85.6 %copy-start.12 = (f32[256]{0:T(256)S(1)}, f32[256]{0:T(256)}, u32[]{:S(2)}) copy-start(f32[256]{0:T(256)} %param.32) | copy-start | bytes 3076
  290.5 85.7 %copy-start.6 = (bf16[4,256]{1,0:T(4,128)(2,1)S(1)}, bf16[4,256]{1,0:T(4,128)(2,1)}, u32[]{:S(2)}) copy-start(bf16[4,256]{1,0:T(4,128)(2,1)} %param.29) | copy-start | bytes 6148
  290.6 99.1 %all-gather.16.cloned.1.call-start = ((), (), s32[]{:S(2)}) async-start(), calls=%async_computation.7 | async-start | bytes 1179648 | tf_op jit(solution)/shard_map/all_gather | solution.py:75
  291.1 223.3 %all-gather.18.cloned.1.call-start = ((), (), s32[]{:S(2)}) async-start(), calls=%async_computation.8 | async-start | bytes 1179648 | tf_op jit(solution)/shard_map/all_gather | solution.py:76
  334.9 14.3 %collective-permute-start.3 = (bf16[1024,512]{1,0:T(8,128)(2,1)S(1)}, bf16[1024,512]{1,0:T(8,128)(2,1)S(1)}, u32[]{:S(2)}, u32[]{:S(2)}) collective-permute-start(bf16[1024,512]{1,0:T(8,128)(2,1)S(1)} %add_convert_fusion.2), channel_id=1, source_target_pairs={{0,1},{1,2},{2,3},{3,0},{4,5},{5,6},{6,7},{7,4},{8,9},{9,10},{10,1... | collective-permute-start | bytes 3145736 | tf_op jit(solution)/shard_map/ppermute | solution.py:23
  334.9 179.5 %all-gather.20.cloned.1.call-start = ((), (), s32[]{:S(2)}) async-start(), calls=%async_computation.9 | async-start | bytes 1179648 | tf_op jit(solution)/shard_map/all_gather | solution.py:77
  349.1 14.3 %collective-permute-start.4 = (bf16[1024,512]{1,0:T(8,128)(2,1)S(1)}, bf16[1024,512]{1,0:T(8,128)(2,1)}, u32[]{:S(2)}, u32[]{:S(2)}) collective-permute-start(bf16[1024,512]{1,0:T(8,128)(2,1)S(1)} %collective-permute-done.3), channel_id=1, source_target_pairs={{0,1},{1,2},{2,3},{3,0},{4,5},{5,6},{6,7},{7,4},{8,9},{9,10},{10,1... | collective-permute-start | bytes 3145736 | tf_op jit(solution)/shard_map/ppermute | solution.py:23
  363.5 14.5 %collective-permute-start.5 = (bf16[1024,512]{1,0:T(8,128)(2,1)}, bf16[1024,512]{1,0:T(8,128)(2,1)}, u32[]{:S(2)}, u32[]{:S(2)}) collective-permute-start(bf16[1024,512]{1,0:T(8,128)(2,1)} %collective-permute-done.4), channel_id=1, source_target_pairs={{0,1},{1,2},{2,3},{3,0},{4,5},{5,6},{6,7},{7,4},{8,9},{9,10},{10,1... | collective-permute-start | bytes 3145736 | tf_op jit(solution)/shard_map/ppermute | solution.py:23
  363.5 205.1 %reduce-scatter.6.cloned.1.call-start = ((), (), s32[]{:S(2)}) async-start(), calls=%async_computation.10 | async-start | bytes 5242880 | tf_op jit(solution)/shard_map/reduce_scatter | solution.py:31
  374.8 14.9 %copy-start.15 = (f32[2048]{0:T(1024)S(1)}, f32[2048]{0:T(1024)}, u32[]{:S(2)}) copy-start(f32[2048]{0:T(1024)} %param.26) | copy-start | bytes 24580
  502.3 11.8 %copy-start.4 = (f32[1,511,256]{2,1,0:T(8,128)S(1)}, f32[1,511,256]{2,1,0:T(8,128)}, u32[]{:S(2)}) copy-start(f32[1,511,256]{2,1,0:T(8,128)} %slice.261) | copy-start | bytes 1569796
  524.1 132.7 %all-gather.22.cloned.1.call-start = ((), (), s32[]{:S(2)}) async-start(), calls=%async_computation.11 | async-start | bytes 5898240 | tf_op jit(solution)/shard_map/all_gather | solution.py:45
  524.8 218.1 %all-gather.24.cloned.1.call-start = ((), (), s32[]{:S(2)}) async-start(), calls=%async_computation.12 | async-start | bytes 5898240 | tf_op jit(solution)/shard_map/all_gather | solution.py:46
  525.4 303.8 %all-gather.26.cloned.1.call-start = ((), (), s32[]{:S(2)}) async-start(), calls=%async_computation.13 | async-start | bytes 5898240 | tf_op jit(solution)/shard_map/all_gather | solution.py:47
  526.1 130.6 %copy-start.17 = (f32[2048]{0:T(1024)S(1)}, f32[2048]{0:T(1024)}, u32[]{:S(2)}) copy-start(f32[2048]{0:T(1024)} %param.35) | copy-start | bytes 24580
  526.1 365.6 %reduce-scatter.8.cloned.1.call-start = ((), (), s32[]{:S(2)}) async-start(), calls=%async_computation.14 | async-start | bytes 5242880 | tf_op jit(solution)/shard_map/reduce_scatter | solution.py:31
  570.1 14.3 %collective-permute-start.6 = (bf16[1024,512]{1,0:T(8,128)(2,1)S(1)}, bf16[1024,512]{1,0:T(8,128)(2,1)S(1)}, u32[]{:S(2)}, u32[]{:S(2)}) collective-permute-start(bf16[1024,512]{1,0:T(8,128)(2,1)S(1)} %add_convert_fusion.1), channel_id=1, source_target_pairs={{0,1},{1,2},{2,3},{3,0},{4,5},{5,6},{6,7},{7,4},{8,9},{9,10},{10,1... | collective-permute-start | bytes 3145736 | tf_op jit(solution)/shard_map/ppermute | solution.py:23
  584.4 14.2 %collective-permute-start.7 = (bf16[1024,512]{1,0:T(8,128)(2,1)S(1)}, bf16[1024,512]{1,0:T(8,128)(2,1)S(1)}, u32[]{:S(2)}, u32[]{:S(2)}) collective-permute-start(bf16[1024,512]{1,0:T(8,128)(2,1)S(1)} %collective-permute-done.6), channel_id=1, source_target_pairs={{0,1},{1,2},{2,3},{3,0},{4,5},{5,6},{6,7},{7,4},{8,9},{9,10},{10,1... | collective-permute-start | bytes 3145736 | tf_op jit(solution)/shard_map/ppermute | solution.py:23
  598.6 14.2 %collective-permute-start.8 = (bf16[1024,512]{1,0:T(8,128)(2,1)S(1)}, bf16[1024,512]{1,0:T(8,128)(2,1)S(1)}, u32[]{:S(2)}, u32[]{:S(2)}) collective-permute-start(bf16[1024,512]{1,0:T(8,128)(2,1)S(1)} %collective-permute-done.7), channel_id=1, source_target_pairs={{0,1},{1,2},{2,3},{3,0},{4,5},{5,6},{6,7},{7,4},{8,9},{9,10},{10,1... | collective-permute-start | bytes 3145736 | tf_op jit(solution)/shard_map/ppermute | solution.py:23
  829.2 72.7 %copy-start.1 = (bf16[4,64,64]{2,1,0:T(8,128)(2,1)S(1)}, bf16[4,64,64]{2,1,0:T(8,128)(2,1)}, u32[]{:S(2)}) copy-start(bf16[4,64,64]{2,1,0:T(8,128)(2,1)} %param.30) | copy-start | bytes 98308
  849.0 50.3 %copy-start.11 = (f32[512]{0:T(512)S(1)}, f32[512]{0:T(512)}, u32[]{:S(2)}) copy-start(f32[512]{0:T(512)} %param.39) | copy-start | bytes 6148
  (7 other events, 38.9 us)
Sparse Core Ops, SparseCore 0:
  9.5 88.5 all-gather.9
  100.3 84.0 all-gather.11
  186.6 84.0 all-gather.13
  290.7 42.5 reduce-scatter.3
  335.3 40.2 all-gather.15
  377.6 38.9 all-gather.17
  418.7 38.9 all-gather.19
  524.2 44.3 reduce-scatter.5
  570.8 85.8 all-gather.21
  658.8 84.0 all-gather.23
  745.1 84.0 all-gather.25
  849.1 42.5 reduce-scatter.7
